TPU v7x, 512 devices: a whole 4x8x8 slice. The times are simulated.
512 devices in a mesh: sp: 32 (over z, x), tp: 16 (over y, core).
Axes of the slice: x: 4, y: 8, z: 8, core: 2. Of those that a mesh axis runs over, the one named last changes fastest.
Arguments:
- skip_stream_entering: bfloat16 [4096, 2048], P('sp', 'tp'), may hold values from -24 to 24
- unfiltered_channel_feed: bfloat16 [4096, 2048], P('sp', 'tp'), may hold values from -6 to 6
- unfiltered_state_entry: bfloat16 [4096, 2048], P('sp', 'tp'), may hold values from -6 to 6
- unfiltered_state_exit: bfloat16 [4096, 2048], P('sp', 'tp'), may hold values from -6 to 6
- final_valve_preactivation: bfloat16 [4096, 2048], P('sp', 'tp'), may hold values from -6 to 6
- increment_preactivation: float32 [2, 32, 4096], P(None, 'tp', 'sp'), may hold values from -8 to 8
- summed_attenuation_both_ways: float32 [2, 32, 4096], P(None, 'tp', 'sp'), may hold values from -0.7 to 0, as said below
- channel_fading_speed: float32 [2, 32], P(None, 'tp'), may hold values from 4.8828125e-05 to 0.03, as said below
- channel_feed_filter: float32 [5, 2048], P(None, 'tp'), may hold values from -2.5 to 2.5
- state_entry_filter: float32 [5, 2048], P(None, 'tp'), may hold values from -2.5 to 2.5
- state_exit_filter: float32 [5, 2048], P(None, 'tp'), may hold values from -2.5 to 2.5
- clustered_rescale_factor: float32 [2048], P('tp'), may hold values from 0.1 to 1.9
- final_projection_weights: bfloat16 [2048, 2048], P(None, 'tp'), may hold values from -0.125 to 0.125
- specialist_rescale_factor: float32 [2048], replicated, may hold values from 0.1 to 1.9
- item_specialist_couple: int32 [4096, 2], P('sp'), may hold values from 0 to 31, all different within a row; in each aligned block of 128 rows (0 to 127, 128 to 255, ...) at most 16 rows name the same one
- selected_cluster_likelihood: float32 [4096], P('sp'), may hold values from 0.3 to 1
- selected_twin_scores_raw: float32 [4096, 2], P('sp'), may hold values from -6 to 6
- specialist_gating_weights: bfloat16 [32, 2048, 4096], P('sp', None, 'tp'), may hold values from -0.125 to 0.125
- specialist_raising_weights: bfloat16 [32, 2048, 4096], P('sp', None, 'tp'), may hold values from -0.125 to 0.125
- specialist_lowering_weights: bfloat16 [32, 4096, 2048], P('sp', 'tp'), may hold values from -0.09375 to 0.09375
Outputs:
- layer_out: bfloat16 [4096, 2048], P('sp', 'tp')
Inputs may be any that keep to these rules, and one draw needn't show every extreme that they name: For every head, dt times channel_fading_speed at the rate of the draw sets how far a state is carried; summed_attenuation_both_ways holds a few sharp losses of state. `summed_attenuation_both_ways`: mostly zero. `item_specialist_couple`: the two experts of a row differ. Among the rows of one index of sp (aligned blocks of 128 rows) no expert is named by more than 16 rows, a bound that some expert reaches in some blocks.
All inputs are finite; a program needn't handle non-finite values.
Results may differ from a plain program's by a relative error of at most 0.0095.
Values may be sent and summed in bfloat16 or wider, within the bound.
No kernel may reach another device: no remote copies, remote signals or barrier semaphores. Data moves between devices by JAX's collectives and lax.ppermute only.
A program may use at most 64 MiB of HBM per device.

v0:
```python
import jax
import jax.numpy as jnp
from jax import lax
from jax.sharding import Mesh
from jax.sharding import PartitionSpec as P

D = 2048
HD = 64
NS = 128
CONV = 5
SP = ("sp_0", "sp_1")
HIGHEST = lax.Precision.HIGHEST
group_eps = 1e-05
stream_eps = 1e-06


def extended(cells, sides, width):
    for axis, dim in sides:
        count = lax.axis_size(axis)
        ends = count - 1
        head = lax.slice_in_dim(cells, 0, width, axis=dim)
        tail = lax.slice_in_dim(cells, cells.shape[dim] - width, cells.shape[dim], axis=dim)
        cells = jnp.concatenate(
            [
                lax.ppermute(tail, axis, [(i, (i + 1) % count) for i in range(ends)]),
                cells,
                lax.ppermute(head, axis, [((i + 1) % count, i) for i in range(ends)]),
            ],
            axis=dim,
        )
    return cells


def filled_with(shard, identity):
    return jax.tree.map(
        lambda a, e: jnp.broadcast_to(jnp.asarray(e, a.dtype), a.shape), shard, identity
    )


def all_in_one(shard, axis):
    leaves = jax.tree.leaves(shard)
    sequence = sorted(range(len(leaves)), key=lambda k: -leaves[k].size)
    width = (1, *leaves[sequence[0]].shape)[-1]
    lines = [
        jnp.pad(leaves[k].reshape(-1), (0, -leaves[k].size % width)).reshape(-1, width)
        for k in sequence
    ]
    both, at, found = (lax.all_gather(jnp.concatenate(lines), axis), 0, {})
    for k, line in zip(sequence, lines):
        share = both[:, at : at + len(line)].reshape(len(both), -1)
        found[k] = share[:, : leaves[k].size].reshape(-1, *leaves[k].shape)
        at += len(line)
    numbers = iter(range(len(leaves)))
    return jax.tree.map(lambda _: found[next(numbers)], shard)


def carried_in(shard, axes, combine, identity, reverse):
    before = start = filled_with(shard, identity)
    so_far = shard
    for axis in reversed(axes):
        peers, mine = (lax.axis_size(axis), lax.axis_index(axis))
        pieces = all_in_one(
            jax.tree.map(
                lambda part, kind: part.astype(kind), so_far, (jnp.bfloat16, jnp.bfloat16)
            ),
            axis,
        )
        inside, so_far = (start, start)
        for k in reversed(range(peers)) if reverse else range(peers):
            passed = k > mine if reverse else k < mine
            so_far = combine(
                so_far, jax.tree.map(lambda part, own: part[k].astype(own.dtype), pieces, shard)
            )
            inside = jax.tree.map(lambda new, old: jnp.where(passed, new, old), so_far, inside)
        before = combine(inside, before)
    return before


def in_blocks(shard, dim, peers):
    shape = shard.shape
    parts = shard.reshape(*shape[:dim], peers, shape[dim] // peers, *shape[dim + 1 :])
    return jnp.moveaxis(parts, dim, 0)


def sum_at_owner(shard, axis, dim):
    peers = lax.axis_size(axis)
    parts = lax.all_to_all(in_blocks(shard, dim, peers), axis, 0, 0, tiled=True)
    return jnp.sum(parts.astype(jnp.float32), axis=0)


def block_parts(x_short, b_short, c_short, step_f, step_b, log_f, log_b):
    head_count = x_short.shape[1]
    group_count = b_short.shape[1]
    per_group = head_count // group_count
    length = x_short.shape[0]
    group_scores = jnp.einsum("tgn,sgn->gts", c_short, b_short, preferred_element_type=jnp.float32)
    x_block = x_short.astype(jnp.float32)
    b_block = b_short.astype(jnp.float32)
    c_block = c_short.astype(jnp.float32)
    scores = jnp.repeat(group_scores, per_group, axis=0)
    b_head = jnp.repeat(b_block, per_group, axis=1)
    c_head = jnp.repeat(c_block, per_group, axis=1)
    forward = jnp.cumsum(log_f, axis=1)
    backward = jnp.flip(jnp.cumsum(jnp.flip(log_b, 1), axis=1), 1)
    row_index = lax.broadcasted_iota(jnp.int32, (length, length), 0)
    col_index = lax.broadcasted_iota(jnp.int32, (length, length), 1)
    lower_mask = (col_index <= row_index)[None]
    upper_mask = (col_index >= row_index)[None]
    decay_fwd = jnp.where(
        lower_mask, jnp.exp(jnp.minimum(forward[:, :, None] - forward[:, None, :], 0.0)), 0.0
    )
    decay_bwd = jnp.where(
        upper_mask, jnp.exp(jnp.minimum(backward[:, :, None] - backward[:, None, :], 0.0)), 0.0
    )
    mixing = scores * (decay_fwd * step_f[:, None, :] + decay_bwd * step_b[:, None, :])
    within = jnp.einsum("hts,shp->thp", mixing, x_block, precision=HIGHEST)
    weight_fwd = jnp.exp(forward[:, -1:] - forward) * step_f
    weight_bwd = jnp.exp(backward[:, :1] - backward) * step_b
    state_fwd = jnp.einsum("hs,shp,shn->hpn", weight_fwd, x_block, b_head, precision=HIGHEST)
    state_bwd = jnp.einsum("hs,shp,shn->hpn", weight_bwd, x_block, b_head, precision=HIGHEST)
    return (
        within,
        state_fwd,
        state_bwd,
        forward[:, -1],
        backward[:, 0],
        jnp.exp(forward),
        jnp.exp(backward),
        c_head,
    )


def read_state(c_head, factor, state):
    return (
        jnp.einsum("thn,hpn->thp", c_head, state, precision=HIGHEST)
        * jnp.transpose(factor)[:, :, None]
    )


def compose(earlier, later):
    return (earlier[0] + later[0], earlier[1] * jnp.exp(later[0])[:, None, None] + later[1])


def body(
    skip_stream_entering,
    unfiltered_channel_feed,
    unfiltered_state_entry,
    unfiltered_state_exit,
    final_valve_preactivation,
    increment_preactivation,
    summed_attenuation_both_ways,
    channel_fading_speed,
    channel_feed_filter,
    state_entry_filter,
    state_exit_filter,
    clustered_rescale_factor,
    final_projection_weights,
    specialist_rescale_factor,
    item_specialist_couple,
    selected_cluster_likelihood,
    selected_twin_scores_raw,
    specialist_gating_weights,
    specialist_raising_weights,
    specialist_lowering_weights,
):
    tokens_here = skip_stream_entering.shape[0]
    heads_here = increment_preactivation.shape[1]
    x_width = unfiltered_channel_feed.shape[1]
    b_width = unfiltered_state_entry.shape[1]
    groups_here = b_width // NS
    joined = jnp.concatenate(
        [unfiltered_channel_feed, unfiltered_state_entry, unfiltered_state_exit], axis=1
    )
    padded = extended(joined, ((SP, 0),), CONV // 2)
    kernel = jnp.concatenate([channel_feed_filter, state_entry_filter, state_exit_filter], axis=1)
    summed = jnp.zeros(joined.shape, jnp.float32)
    for offset in range(CONV):
        summed = summed + kernel[offset] * padded[offset : offset + tokens_here].astype(jnp.float32)
    conv_out = jax.nn.silu(summed).astype(jnp.bfloat16)
    x_conv = conv_out[:, :x_width].reshape(tokens_here, heads_here, HD)
    b_conv = conv_out[:, x_width : x_width + b_width].reshape(tokens_here, groups_here, NS)
    c_conv = conv_out[:, x_width + b_width :].reshape(tokens_here, groups_here, NS)
    whole_increment_list = jax.nn.softplus(increment_preactivation)
    whole_attenuation_list = (
        -whole_increment_list * channel_fading_speed[:, :, None] + summed_attenuation_both_ways
    )
    within, state_fwd, state_bwd, total_fwd, total_bwd, factor_fwd, factor_bwd, c_head = (
        block_parts(
            x_conv,
            b_conv,
            c_conv,
            whole_increment_list[0],
            whole_increment_list[1],
            whole_attenuation_list[0],
            whole_attenuation_list[1],
        )
    )
    empty = (jnp.zeros_like(total_fwd), jnp.zeros_like(state_fwd))
    incoming_fwd = carried_in((total_fwd, state_fwd), SP, compose, empty, False)[1]
    incoming_bwd = carried_in((total_bwd, state_bwd), SP, compose, empty, True)[1]
    mixer_out = (
        within
        + read_state(c_head, factor_fwd, incoming_fwd)
        + read_state(c_head, factor_bwd, incoming_bwd)
    )
    gated = mixer_out.reshape(tokens_here, x_width) * jax.nn.silu(
        final_valve_preactivation.astype(jnp.float32)
    )
    grouped = gated.reshape(tokens_here, groups_here, -1)
    grouped = grouped * lax.rsqrt(jnp.mean(grouped * grouped, axis=-1, keepdims=True) + group_eps)
    mixed = (grouped.reshape(tokens_here, x_width) * clustered_rescale_factor).astype(jnp.bfloat16)
    projected = jnp.dot(
        lax.all_gather(mixed, "tp", axis=1, tiled=True),
        final_projection_weights,
        preferred_element_type=jnp.float32,
    )
    stream = (skip_stream_entering.astype(jnp.float32) + projected).astype(jnp.bfloat16)
    stream_f = stream.astype(jnp.float32)
    col_count = skip_stream_entering.shape[1]
    whole_rows = lax.all_gather(stream, "tp", axis=1, tiled=True).astype(jnp.float32)
    normal_rows = (
        whole_rows
        * lax.rsqrt(jnp.mean(whole_rows * whole_rows, axis=-1, keepdims=True) + stream_eps)
        * specialist_rescale_factor
    ).astype(jnp.bfloat16)
    expert_total = lax.axis_size(SP)
    capacity = 4 * tokens_here // expert_total
    flat_ids = item_specialist_couple.reshape(-1)
    assignments = flat_ids.shape[0]
    expert_iota = lax.broadcasted_iota(jnp.int32, (assignments, expert_total), 1)
    one_hot = (flat_ids[:, None] == expert_iota).astype(jnp.int32)
    ranking = jnp.sum((jnp.cumsum(one_hot, axis=0) - 1) * one_hot, axis=1)
    slot_index = flat_ids * capacity + ranking
    slot_iota = lax.broadcasted_iota(jnp.int32, (expert_total * capacity, assignments), 0)
    selector = (slot_index[None, :] == slot_iota).astype(jnp.bfloat16)
    selector = jnp.sum(selector.reshape(expert_total * capacity, tokens_here, -1), axis=2)
    weight_gate = specialist_gating_weights[0]
    weight_up = specialist_raising_weights[0]
    weight_down = specialist_lowering_weights[0]
    outgoing = jnp.dot(selector, normal_rows, preferred_element_type=jnp.float32).astype(
        jnp.bfloat16
    )
    outgoing = outgoing.reshape(expert_total, capacity, D)
    arrived = lax.all_to_all(outgoing, SP, split_axis=0, concat_axis=0, tiled=True)
    sources = arrived.shape[0]
    slot_count = arrived.shape[1]
    rows = arrived.reshape(sources * slot_count, arrived.shape[2])
    gate = jnp.dot(rows, weight_gate, preferred_element_type=jnp.float32)
    upward = jnp.dot(rows, weight_up, preferred_element_type=jnp.float32)
    hidden = (jax.nn.silu(gate) * upward).astype(jnp.bfloat16)
    partial_out = jnp.dot(hidden, weight_down, preferred_element_type=jnp.float32).astype(
        jnp.bfloat16
    )
    partial_out = partial_out.reshape(sources, slot_count, partial_out.shape[1])
    expert_cols = sum_at_owner(partial_out, "tp", 2).astype(jnp.bfloat16)
    returned = lax.all_to_all(expert_cols, SP, split_axis=0, concat_axis=0, tiled=True)
    flat_back = returned.reshape(expert_total * capacity, col_count)
    picked = (
        jnp.take(flat_back, slot_index, axis=0)
        .astype(jnp.float32)
        .reshape(tokens_here, -1, col_count)
    )
    first = jax.nn.sigmoid(selected_twin_scores_raw[:, 0] - selected_twin_scores_raw[:, 1])
    route_weight = selected_cluster_likelihood[:, None] * jnp.stack([first, 1.0 - first], axis=1)
    experts_sum = jnp.sum(route_weight[:, :, None] * picked, axis=1)
    return (stream_f + experts_sum).astype(jnp.bfloat16)


def solution(mesh):
    torus = Mesh(mesh.devices.reshape(8, 4, mesh.shape["tp"]), ("sp_0", "sp_1", "tp"))
    return jax.shard_map(
        body,
        mesh=torus,
        in_specs=(
            P(SP, "tp"),
            P(SP, "tp"),
            P(SP, "tp"),
            P(SP, "tp"),
            P(SP, "tp"),
            P(None, "tp", SP),
            P(None, "tp", SP),
            P(None, "tp"),
            P(None, "tp"),
            P(None, "tp"),
            P(None, "tp"),
            P("tp"),
            P(None, "tp"),
            P(),
            P(SP, None),
            P(SP),
            P(SP, None),
            P(SP, None, "tp"),
            P(SP, None, "tp"),
            P(SP, "tp", None),
        ),
        out_specs=P(SP, "tp"),
        check_vma=False,
    )
```

profile of v0, /device:TPU:1, one launch (start us, length us, event | category | flops | bytes accessed | tf_op | source)
XLA Modules:
  0.0 280.2 jit_solution(5651927392031734438)
XLA Ops:
  0.0 0.9 constant_dynamic-update-slice_fusion.5
  0.9 0.8 constant_dynamic-update-slice_fusion.4
  1.6 0.8 constant_dynamic-update-slice_fusion.3
  2.4 3.9 %collective-permute-start = (bf16[2,384]{1,0:T(2,128)(2,1)S(1)}, bf16[2,384]{1,0:T(2,128)(2,1)S(1)}, u32[]{:S(2)}, u32[]{:S(2)}) collective-permute-start(bf16[2,384]{1,0:T(2,128)(2,1)S(1)} %get-tuple-element.47), channel_id=1, source_target_pairs={{0,16},{16,32},{32,48},{48,64},{64,80},{80,96},{96,112},{112,128},... | collective-permute-start | bytes 4616 | tf_op jit(solution)/shard_map/ppermute | solution.py:25
  6.3 1.3 collective-permute-start.1
  7.7 0.8 copy.71
  8.8 0.8 multiply_add_fusion
  10.7 0.7 constant_dynamic-update-slice_fusion.2
  11.4 0.7 constant_dynamic-update-slice_fusion.1
  12.1 0.7 constant_dynamic-update-slice_fusion
  12.8 0.6 reduce-window.6
  14.0 0.7 compare_and_fusion
  15.4 10.4 %all-gather.6 = bf16[4,129,128]{2,1,0:T(8,128)(2,1)S(1)} all-gather(bf16[1,129,128]{2,1,0:T(8,128)(2,1)S(1)} %maximum_bitcast_fusion.2), channel_id=4, replica_groups=mesh['sp_0'=8,'sp_1'=4,'tp'=16] {'sp_1'}, dimensions={0}, use_global_device_ids=true | all-gather | bytes 165120 | tf_op jit(solution)/shard_map/all_gather | solution.py:48
  26.6 27.4 %all-gather.7 = bf16[8,129,128]{2,1,0:T(8,128)(2,1)S(1)} all-gather(bf16[1,129,128]{2,1,0:T(8,128)(2,1)S(1)} %maximum_bitcast_fusion.3), channel_id=5, replica_groups=mesh['sp_0'=8,'sp_1'=4,'tp'=16] {'sp_0'}, dimensions={0}, use_global_device_ids=true | all-gather | bytes 297216 | tf_op jit(solution)/shard_map/all_gather | solution.py:48
  54.2 9.1 %all-gather.4 = bf16[4,129,128]{2,1,0:T(8,128)(2,1)S(1)} all-gather(bf16[1,129,128]{2,1,0:T(8,128)(2,1)S(1)} %maximum_bitcast_fusion), channel_id=2, replica_groups=mesh['sp_0'=8,'sp_1'=4,'tp'=16] {'sp_1'}, dimensions={0}, use_global_device_ids=true | all-gather | bytes 165120 | tf_op jit(solution)/shard_map/all_gather | solution.py:48
  64.2 18.5 %all-gather.5 = bf16[8,129,128]{2,1,0:T(8,128)(2,1)S(1)} all-gather(bf16[1,129,128]{2,1,0:T(8,128)(2,1)S(1)} %maximum_bitcast_fusion.1), channel_id=3, replica_groups=mesh['sp_0'=8,'sp_1'=4,'tp'=16] {'sp_0'}, dimensions={0}, use_global_device_ids=true | all-gather | bytes 297216 | tf_op jit(solution)/shard_map/all_gather | solution.py:48
  83.4 0.5 fusion.5
  84.8 37.9 %all_gather.38 = bf16[128,2048]{1,0:T(8,128)(2,1)S(1)} all-gather(bf16[128,128]{1,0:T(8,128)(2,1)S(1)} %multiply_convert_fusion.1), channel_id=1, replica_groups=mesh['sp_0'=8,'sp_1'=4,'tp'=16] {'tp'}, dimensions={1}, use_global_device_ids=true | all-gather | bytes 557056 | tf_op jit(solution)/shard_map/all_gather | solution.py:213
  123.0 16.4 %all_gather.39 = bf16[128,2048]{1,0:T(8,128)(2,1)S(1)} all-gather(bf16[128,128]{1,0:T(8,128)(2,1)S(1)} %fusion.6), channel_id=1, replica_groups=mesh['sp_0'=8,'sp_1'=4,'tp'=16] {'tp'}, dimensions={1}, use_global_device_ids=true | all-gather | bytes 557056 | tf_op jit(solution)/shard_map/all_gather | solution.py:220
  139.6 0.8 convolution_convert_fusion.1
  140.4 55.6 %all_to_all.15 = bf16[32,16,2048]{2,1,0:T(8,128)(2,1)S(1)} all-to-all(bf16[32,16,2048]{2,1,0:T(8,128)(2,1)S(1)} %bitcast.252), channel_id=1, replica_groups=mesh['sp_0'=8,'sp_1'=4,'tp'=16] {'sp_0','sp_1'}, dimensions={0} | all-to-all | bytes 4194304 | tf_op jit(solution)/shard_map/all_to_all | solution.py:244
  196.0 1.5 fusion.12
  197.5 5.0 %fusion = bf16[64,8,16,128]{3,1,2,0:T(8,128)(2,1)} fusion(bf16[1,256,2048]{2,1,0:T(8,128)(2,1)S(1)} %copy-done, bf16[512,2048]{1,0:T(8,128)(2,1)S(1)} %bitcast.256, bf16[1,2048,256]{2,1,0:T(8,128)(2,1)} %param.38, f32[512,256]{1,0:T(8,128)} %fusion.12), kind=kOutput, calls=%fused_computation.4 | convolution fusion | flops 1075576832 | bytes 6815744 | tf_op jit(solution)/shard_map/dot_general | solution.py:251
  202.6 2.2 copy.83
  204.8 1.9 copy.90
  206.7 6.9 %all-to-all-start.1 = ((bf16[16,32,16,128]{3,2,1,0:T(8,128)(2,1)}), bf16[16,32,16,128]{3,2,1,0:T(8,128)(2,1)S(1)}, u32[]{:S(2)}, u32[]{:S(2)}) async-start(bf16[16,32,16,128]{3,2,1,0:T(8,128)(2,1)} %bitcast.251), calls=%async_computation.1 | async-start | bytes 4194304 | tf_op jit(solution)/shard_map/all_to_all | solution.py:87
  214.2 48.5 %all-to-all-done.1 = bf16[16,32,16,128]{3,2,1,0:T(8,128)(2,1)S(1)} async-done(((bf16[16,32,16,128]{3,2,1,0:T(8,128)(2,1)}), bf16[16,32,16,128]{3,2,1,0:T(8,128)(2,1)S(1)}, u32[]{:S(2)}, u32[]{:S(2)}) %all-to-all-start.1) | async-done | bytes 2097184 | tf_op jit(solution)/shard_map/all_to_all | solution.py:87
  262.6 0.9 reduce_sum.69
  263.6 5.3 %all-to-all-start.2 = ((bf16[32,16,128]{2,1,0:T(8,128)(2,1)}), bf16[32,16,128]{2,1,0:T(8,128)(2,1)S(1)}, u32[]{:S(2)}, u32[]{:S(2)}) async-start(bf16[32,16,128]{2,1,0:T(8,128)(2,1)} %reduce_sum.69), calls=%async_computation.2 | async-start | bytes 262144 | tf_op jit(solution)/shard_map/all_to_all | solution.py:256
  268.9 9.4 %all-to-all-done.2 = bf16[32,16,128]{2,1,0:T(8,128)(2,1)S(1)} async-done(((bf16[32,16,128]{2,1,0:T(8,128)(2,1)}), bf16[32,16,128]{2,1,0:T(8,128)(2,1)S(1)}, u32[]{:S(2)}, u32[]{:S(2)}) %all-to-all-start.2) | async-done | bytes 131104 | tf_op jit(solution)/shard_map/all_to_all | solution.py:256
  278.3 0.9 gather_fusion
  279.6 0.6 add_convert_fusion
  (114 shorter events, 7.3 us)
Async XLA Ops:
  0.0 197.5 %copy-start = (bf16[1,256,2048]{2,1,0:T(8,128)(2,1)S(1)}, bf16[1,256,2048]{2,1,0:T(8,128)(2,1)}, u32[]{:S(2)}) copy-start(bf16[1,256,2048]{2,1,0:T(8,128)(2,1)} %param.39) | copy-start | bytes 3145732
  2.4 12.4 %collective-permute-start = (bf16[2,384]{1,0:T(2,128)(2,1)S(1)}, bf16[2,384]{1,0:T(2,128)(2,1)S(1)}, u32[]{:S(2)}, u32[]{:S(2)}) collective-permute-start(bf16[2,384]{1,0:T(2,128)(2,1)S(1)} %get-tuple-element.47), channel_id=1, source_target_pairs={{0,16},{16,32},{32,48},{48,64},{64,80},{80,96},{96,112},{112,128},... | collective-permute-start | bytes 4616 | tf_op jit(solution)/shard_map/ppermute | solution.py:25
  6.3 8.4 %collective-permute-start.1 = (bf16[2,384]{1,0:T(2,128)(2,1)S(1)}, bf16[2,384]{1,0:T(2,128)(2,1)S(1)}, u32[]{:S(2)}, u32[]{:S(2)}) collective-permute-start(bf16[2,384]{1,0:T(2,128)(2,1)S(1)} %get-tuple-element.48), channel_id=1, source_target_pairs={{16,0},{32,16},{48,32},{64,48},{80,64},{96,80},{112,96},{128,112},... | collective-permute-start | bytes 4616 | tf_op jit(solution)/shard_map/ppermute | solution.py:27
  82.7 1.9 copy-start.2
  82.7 2.0 copy-start.7
  82.7 40.0 %copy-start.1 = (bf16[2048,128]{1,0:T(8,128)(2,1)S(1)}, bf16[2048,128]{1,0:T(8,128)(2,1)}, u32[]{:S(2)}) copy-start(bf16[2048,128]{1,0:T(8,128)(2,1)} %param.32) | copy-start | bytes 1572868
  82.7 40.0 %copy-start.3 = (bf16[128,128]{1,0:T(8,128)(2,1)S(1)}, bf16[128,128]{1,0:T(8,128)(2,1)}, u32[]{:S(2)}) copy-start(bf16[128,128]{1,0:T(8,128)(2,1)} %param.20) | copy-start | bytes 98308
  83.9 55.7 %copy-start.5 = (f32[2048]{0:T(1024)S(1)}, f32[2048]{0:T(1024)}, u32[]{:S(2)}) copy-start(f32[2048]{0:T(1024)} %param.33) | copy-start | bytes 24580
  140.4 55.6 %copy-start.9 = (bf16[1,2048,256]{2,1,0:T(8,128)(2,1)S(1)}, bf16[1,2048,256]{2,1,0:T(8,128)(2,1)}, u32[]{:S(2)}) copy-start(bf16[1,2048,256]{2,1,0:T(8,128)(2,1)} %param.37) | copy-start | bytes 3145732
  206.7 6.9 %copy-start.4 = (s32[128,2]{0,1:T(2,128)S(1)}, s32[128,2]{0,1:T(2,128)}, u32[]{:S(2)}) copy-start(s32[128,2]{0,1:T(2,128)} %param.34) | copy-start | bytes 3076
  206.7 7.3 %copy-start.6 = (f32[128,2]{0,1:T(2,128)S(1)}, f32[128,2]{0,1:T(2,128)}, u32[]{:S(2)}) copy-start(f32[128,2]{0,1:T(2,128)} %param.36) | copy-start | bytes 3076
  206.7 7.4 %copy-start.8 = (f32[128]{0:T(128)S(1)}, f32[128]{0:T(128)}, u32[]{:S(2)}) copy-start(f32[128]{0:T(128)} %param.35) | copy-start | bytes 1540
  206.7 56.0 %all-to-all-start.1 = ((bf16[16,32,16,128]{3,2,1,0:T(8,128)(2,1)}), bf16[16,32,16,128]{3,2,1,0:T(8,128)(2,1)S(1)}, u32[]{:S(2)}, u32[]{:S(2)}) async-start(bf16[16,32,16,128]{3,2,1,0:T(8,128)(2,1)} %bitcast.251), calls=%async_computation.1 | async-start | bytes 4194304 | tf_op jit(solution)/shard_map/all_to_all | solution.py:87
  263.6 14.8 %all-to-all-start.2 = ((bf16[32,16,128]{2,1,0:T(8,128)(2,1)}), bf16[32,16,128]{2,1,0:T(8,128)(2,1)S(1)}, u32[]{:S(2)}, u32[]{:S(2)}) async-start(bf16[32,16,128]{2,1,0:T(8,128)(2,1)} %reduce_sum.69), calls=%async_computation.2 | async-start | bytes 262144 | tf_op jit(solution)/shard_map/all_to_all | solution.py:256
where the time goes:
time: 281 us; the launch traced here: 280 us
  blocking collectives  175 us (62%)
  waiting for transfers between devices  57.9 us (21%)
  starting transfers between devices  17.4 us (6%)
  local copies, waits for them, and re-layouts  13.4 us (5%)
  matrix products  9.61 us (3%)
  other arithmetic  6.01 us (2%)
    all_gather x4, blocking collectives, all_in_one(): both, at, found = (lax.all_gather(jnp.concatenate(lines), axis), 0, {})  65.3 us
    all_to_all x1, blocking collectives, body(): lax.all_to_all(outgoing, SP, split_axis=0, concat_axis=0, tiled=True)  55.6 us
    all_to_all x1, waiting for transfers between devices, sum_at_owner(): parts = lax.all_to_all(in_blocks(shard, dim, peers), axis, 0, 0, tiled=True)  48.5 us
    all_gather x1, blocking collectives, body(): lax.all_gather(mixed, 'tp', axis=1, tiled=True)  37.9 us
    all_gather x1, blocking collectives, body(): lax.all_gather(stream, 'tp', axis=1, tiled=True).astype(jnp.float32)  16.4 us
    all_to_all x1, waiting for transfers between devices, body(): lax.all_to_all(expert_cols, SP, split_axis=0, concat_axis=0, tiled=True)  9.43 us
    all_to_all x1, starting transfers between devices, sum_at_owner(): parts = lax.all_to_all(in_blocks(shard, dim, peers), axis, 0, 0, tiled=True)  6.91 us
    unnamed x30, local copies, waits for them, and re-layouts  6.06 us
  transfers between devices with their start and end apart: 4, of which 2 were waited for; matrix products, arithmetic and copies ran while one was open for 3% of the time, Pallas kernels for 0%

commit v1 on v0

--- a/solution.py
+++ b/solution.py
@@ -12,6 +12,10 @@
 HIGHEST = lax.Precision.HIGHEST
 group_eps = 1e-05
 stream_eps = 1e-06
+produce_state = lambda vector, row_axis: jnp.concatenate(
+    lax.all_to_all(jnp.stack([vector for _ in range(lax.axis_size(row_axis))]), row_axis, 0, 0),
+    axis=1,
+)
 
 
 def extended(cells, sides, width):
@@ -217,7 +221,7 @@
     stream = (skip_stream_entering.astype(jnp.float32) + projected).astype(jnp.bfloat16)
     stream_f = stream.astype(jnp.float32)
     col_count = skip_stream_entering.shape[1]
-    whole_rows = lax.all_gather(stream, "tp", axis=1, tiled=True).astype(jnp.float32)
+    whole_rows = produce_state(stream, "tp").astype(jnp.float32)
     normal_rows = (
         whole_rows
         * lax.rsqrt(jnp.mean(whole_rows * whole_rows, axis=-1, keepdims=True) + stream_eps)

time: 281 us -> 282 us (level)
  waiting for transfers between devices: 57.9 us -> 73.5 us
  blocking collectives: 175 us -> 160 us
    all_gather x1 -> x0, blocking collectives: 16.4 us -> none  [body(): lax.all_gather(stream, 'tp', axis=1, tiled=True).astype(jnp.float32)]
    all_to_all x0 -> x1, waiting for transfers between devices: none -> 15.6 us  [lax.all_to_all(jnp.stack([vector for _ in range(lax.axis_size(row_axis))]...]
    all_to_all x0 -> x1, starting transfers between devices: none -> 4.49 us  [lax.all_to_all(jnp.stack([vector for _ in range(lax.axis_size(row_axis))]...]
    all_to_all x1, starting transfers between devices: 6.91 us -> 4.03 us  [sum_at_owner(): parts = lax.all_to_all(in_blocks(shard, dim, peers), axis, 0, 0, tiled=True)]
  transfers between devices with their start and end apart: 4 -> 5, of which waited for: 2 -> 3; matrix products, arithmetic and copies ran while one was open for 3% -> 2% of each run, Pallas kernels for 0% -> 0%
where the time goes in v1:
time: 282 us
  blocking collectives  160 us (57%)
  waiting for transfers between devices  73.5 us (26%)
  starting transfers between devices  18.9 us (7%)
  local copies, waits for them, and re-layouts  13.7 us (5%)
  matrix products  9.54 us (3%)
  other arithmetic  5.76 us (2%)
    all_gather x4, blocking collectives, all_in_one(): both, at, found = (lax.all_gather(jnp.concatenate(lines), axis), 0, {})  65.6 us
    all_to_all x1, blocking collectives, body(): lax.all_to_all(outgoing, SP, split_axis=0, concat_axis=0, tiled=True)  56.4 us
    all_to_all x1, waiting for transfers between devices, sum_at_owner(): parts = lax.all_to_all(in_blocks(shard, dim, peers), axis, 0, 0, tiled=True)  48.5 us
    all_gather x1, blocking collectives, body(): lax.all_gather(mixed, 'tp', axis=1, tiled=True)  37.5 us
    all_to_all x1, waiting for transfers between devices, lax.all_to_all(jnp.stack([vector for _ in range(lax.axis_size(row_axis))]...  15.6 us
    all_to_all x1, waiting for transfers between devices, body(): lax.all_to_all(expert_cols, SP, split_axis=0, concat_axis=0, tiled=True)  9.43 us
  transfers between devices with their start and end apart: 5, of which 3 were waited for; matrix products, arithmetic and copies ran while one was open for 2% of the time, Pallas kernels for 0%

profile of v1, /device:TPU:1, one launch (start us, length us, event | category | flops | bytes accessed | tf_op | source)
XLA Modules:
  0.0 281.6 jit_solution(8827319356396818228)
XLA Ops:
  0.0 0.9 constant_dynamic-update-slice_fusion.5
  0.9 0.8 constant_dynamic-update-slice_fusion.4
  1.6 0.8 constant_dynamic-update-slice_fusion.3
  2.4 3.9 %collective-permute-start = (bf16[2,384]{1,0:T(2,128)(2,1)S(1)}, bf16[2,384]{1,0:T(2,128)(2,1)S(1)}, u32[]{:S(2)}, u32[]{:S(2)}) collective-permute-start(bf16[2,384]{1,0:T(2,128)(2,1)S(1)} %get-tuple-element.47), channel_id=1, source_target_pairs={{0,16},{16,32},{32,48},{48,64},{64,80},{80,96},{96,112},{112,128},... | collective-permute-start | bytes 4616 | tf_op jit(solution)/shard_map/ppermute | solution.py:29
  6.3 1.3 collective-permute-start.1
  7.7 0.8 multiply_add_fusion
  9.6 0.7 constant_dynamic-update-slice_fusion.2
  10.3 0.7 constant_dynamic-update-slice_fusion.1
  11.0 0.7 constant_dynamic-update-slice_fusion
  12.4 10.7 %all-gather.6 = bf16[4,129,128]{2,1,0:T(8,128)(2,1)S(1)} all-gather(bf16[1,129,128]{2,1,0:T(8,128)(2,1)S(1)} %maximum_bitcast_fusion.2), channel_id=4, replica_groups=mesh['sp_0'=8,'sp_1'=4,'tp'=16] {'sp_1'}, dimensions={0}, use_global_device_ids=true | all-gather | bytes 165120 | tf_op jit(solution)/shard_map/all_gather | solution.py:52
  23.9 27.0 %all-gather.7 = bf16[8,129,128]{2,1,0:T(8,128)(2,1)S(1)} all-gather(bf16[1,129,128]{2,1,0:T(8,128)(2,1)S(1)} %maximum_bitcast_fusion.3), channel_id=5, replica_groups=mesh['sp_0'=8,'sp_1'=4,'tp'=16] {'sp_0'}, dimensions={0}, use_global_device_ids=true | all-gather | bytes 297216 | tf_op jit(solution)/shard_map/all_gather | solution.py:52
  51.2 9.1 %all-gather.4 = bf16[4,129,128]{2,1,0:T(8,128)(2,1)S(1)} all-gather(bf16[1,129,128]{2,1,0:T(8,128)(2,1)S(1)} %maximum_bitcast_fusion), channel_id=2, replica_groups=mesh['sp_0'=8,'sp_1'=4,'tp'=16] {'sp_1'}, dimensions={0}, use_global_device_ids=true | all-gather | bytes 165120 | tf_op jit(solution)/shard_map/all_gather | solution.py:52
  61.2 18.8 %all-gather.5 = bf16[8,129,128]{2,1,0:T(8,128)(2,1)S(1)} all-gather(bf16[1,129,128]{2,1,0:T(8,128)(2,1)S(1)} %maximum_bitcast_fusion.1), channel_id=3, replica_groups=mesh['sp_0'=8,'sp_1'=4,'tp'=16] {'sp_0'}, dimensions={0}, use_global_device_ids=true | all-gather | bytes 297216 | tf_op jit(solution)/shard_map/all_gather | solution.py:52
  80.7 0.5 fusion.5
  82.1 37.5 %all_gather.35 = bf16[128,2048]{1,0:T(8,128)(2,1)S(1)} all-gather(bf16[128,128]{1,0:T(8,128)(2,1)S(1)} %multiply_convert_fusion.1), channel_id=1, replica_groups=mesh['sp_0'=8,'sp_1'=4,'tp'=16] {'tp'}, dimensions={1}, use_global_device_ids=true | all-gather | bytes 557056 | tf_op jit(solution)/shard_map/all_gather | solution.py:217
  120.1 0.9 stack.5
  121.0 4.5 %all-to-all-start = ((bf16[16,128,128]{1,2,0:T(8,128)(2,1)}), bf16[16,128,128]{1,2,0:T(8,128)(2,1)S(1)}, u32[]{:S(2)}, u32[]{:S(2)}) async-start(bf16[16,128,128]{1,2,0:T(8,128)(2,1)} %stack.5), calls=%async_computation | async-start | bytes 1048576 | tf_op jit(solution)/shard_map/all_to_all | solution.py:16
  125.9 0.6 reduce-window.6
  127.1 15.6 %all-to-all-done = bf16[16,128,128]{1,2,0:T(8,128)(2,1)S(1)} async-done(((bf16[16,128,128]{1,2,0:T(8,128)(2,1)}), bf16[16,128,128]{1,2,0:T(8,128)(2,1)S(1)}, u32[]{:S(2)}, u32[]{:S(2)}) %all-to-all-start) | async-done | bytes 524320 | tf_op jit(solution)/shard_map/all_to_all | solution.py:16
  143.3 0.7 convolution_convert_fusion.1
  144.0 56.4 %all_to_all.20 = bf16[32,16,2048]{2,1,0:T(8,128)(2,1)S(1)} all-to-all(bf16[32,16,2048]{2,1,0:T(8,128)(2,1)S(1)} %bitcast.261), channel_id=1, replica_groups=mesh['sp_0'=8,'sp_1'=4,'tp'=16] {'sp_0','sp_1'}, dimensions={0} | all-to-all | bytes 4194304 | tf_op jit(solution)/shard_map/all_to_all | solution.py:248
  200.4 1.5 fusion.11
  201.9 5.0 %fusion = bf16[64,8,16,128]{3,1,2,0:T(8,128)(2,1)} fusion(bf16[1,256,2048]{2,1,0:T(8,128)(2,1)S(1)} %copy-done, bf16[512,2048]{1,0:T(8,128)(2,1)S(1)} %bitcast.265, bf16[1,2048,256]{2,1,0:T(8,128)(2,1)} %param.38, f32[512,256]{1,0:T(8,128)} %fusion.11), kind=kOutput, calls=%fused_computation.4 | convolution fusion | flops 1075576832 | bytes 6815744 | tf_op jit(solution)/shard_map/dot_general | solution.py:255
  206.9 2.2 copy.88
  209.2 1.9 copy.95
  211.1 4.0 %all-to-all-start.2 = ((bf16[16,32,16,128]{3,2,1,0:T(8,128)(2,1)}), bf16[16,32,16,128]{3,2,1,0:T(8,128)(2,1)S(1)}, u32[]{:S(2)}, u32[]{:S(2)}) async-start(bf16[16,32,16,128]{3,2,1,0:T(8,128)(2,1)} %bitcast.260), calls=%async_computation.2 | async-start | bytes 4194304 | tf_op jit(solution)/shard_map/all_to_all | solution.py:91
  215.7 48.5 %all-to-all-done.2 = bf16[16,32,16,128]{3,2,1,0:T(8,128)(2,1)S(1)} async-done(((bf16[16,32,16,128]{3,2,1,0:T(8,128)(2,1)}), bf16[16,32,16,128]{3,2,1,0:T(8,128)(2,1)S(1)}, u32[]{:S(2)}, u32[]{:S(2)}) %all-to-all-start.2) | async-done | bytes 2097184 | tf_op jit(solution)/shard_map/all_to_all | solution.py:91
  264.2 0.9 reduce_sum.69
  265.1 5.2 %all-to-all-start.3 = ((bf16[32,16,128]{2,1,0:T(8,128)(2,1)}), bf16[32,16,128]{2,1,0:T(8,128)(2,1)S(1)}, u32[]{:S(2)}, u32[]{:S(2)}) async-start(bf16[32,16,128]{2,1,0:T(8,128)(2,1)} %reduce_sum.69), calls=%async_computation.3 | async-start | bytes 262144 | tf_op jit(solution)/shard_map/all_to_all | solution.py:260
  270.4 9.4 %all-to-all-done.3 = bf16[32,16,128]{2,1,0:T(8,128)(2,1)S(1)} async-done(((bf16[32,16,128]{2,1,0:T(8,128)(2,1)}), bf16[32,16,128]{2,1,0:T(8,128)(2,1)S(1)}, u32[]{:S(2)}, u32[]{:S(2)}) %all-to-all-start.3) | async-done | bytes 131104 | tf_op jit(solution)/shard_map/all_to_all | solution.py:260
  279.8 0.9 gather_fusion
  281.0 0.6 add_convert_fusion
  (118 shorter events, 8.0 us)
Async XLA Ops:
  0.0 201.9 %copy-start = (bf16[1,256,2048]{2,1,0:T(8,128)(2,1)S(1)}, bf16[1,256,2048]{2,1,0:T(8,128)(2,1)}, u32[]{:S(2)}) copy-start(bf16[1,256,2048]{2,1,0:T(8,128)(2,1)} %param.39) | copy-start | bytes 3145732
  2.4 9.4 %collective-permute-start = (bf16[2,384]{1,0:T(2,128)(2,1)S(1)}, bf16[2,384]{1,0:T(2,128)(2,1)S(1)}, u32[]{:S(2)}, u32[]{:S(2)}) collective-permute-start(bf16[2,384]{1,0:T(2,128)(2,1)S(1)} %get-tuple-element.47), channel_id=1, source_target_pairs={{0,16},{16,32},{32,48},{48,64},{64,80},{80,96},{96,112},{112,128},... | collective-permute-start | bytes 4616 | tf_op jit(solution)/shard_map/ppermute | solution.py:29
  6.3 5.5 %collective-permute-start.1 = (bf16[2,384]{1,0:T(2,128)(2,1)S(1)}, bf16[2,384]{1,0:T(2,128)(2,1)S(1)}, u32[]{:S(2)}, u32[]{:S(2)}) collective-permute-start(bf16[2,384]{1,0:T(2,128)(2,1)S(1)} %get-tuple-element.48), channel_id=1, source_target_pairs={{16,0},{32,16},{48,32},{64,48},{80,64},{96,80},{112,96},{128,112},... | collective-permute-start | bytes 4616 | tf_op jit(solution)/shard_map/ppermute | solution.py:31
  80.0 1.9 copy-start.2
  80.0 2.0 copy-start.7
  80.0 39.6 %copy-start.1 = (bf16[2048,128]{1,0:T(8,128)(2,1)S(1)}, bf16[2048,128]{1,0:T(8,128)(2,1)}, u32[]{:S(2)}) copy-start(bf16[2048,128]{1,0:T(8,128)(2,1)} %param.32) | copy-start | bytes 1572868
  80.0 39.6 %copy-start.3 = (bf16[128,128]{1,0:T(8,128)(2,1)S(1)}, bf16[128,128]{1,0:T(8,128)(2,1)}, u32[]{:S(2)}) copy-start(bf16[128,128]{1,0:T(8,128)(2,1)} %param.20) | copy-start | bytes 98308
  81.2 44.2 %copy-start.4 = (s32[128,2]{0,1:T(2,128)S(1)}, s32[128,2]{0,1:T(2,128)}, u32[]{:S(2)}) copy-start(s32[128,2]{0,1:T(2,128)} %param.34) | copy-start | bytes 3076
  119.6 23.3 %copy-start.5 = (f32[2048]{0:T(1024)S(1)}, f32[2048]{0:T(1024)}, u32[]{:S(2)}) copy-start(f32[2048]{0:T(1024)} %param.33) | copy-start | bytes 24580
  121.0 21.7 %all-to-all-start = ((bf16[16,128,128]{1,2,0:T(8,128)(2,1)}), bf16[16,128,128]{1,2,0:T(8,128)(2,1)S(1)}, u32[]{:S(2)}, u32[]{:S(2)}) async-start(bf16[16,128,128]{1,2,0:T(8,128)(2,1)} %stack.5), calls=%async_computation | async-start | bytes 1048576 | tf_op jit(solution)/shard_map/all_to_all | solution.py:16
  144.0 56.4 %copy-start.9 = (bf16[1,2048,256]{2,1,0:T(8,128)(2,1)S(1)}, bf16[1,2048,256]{2,1,0:T(8,128)(2,1)}, u32[]{:S(2)}) copy-start(bf16[1,2048,256]{2,1,0:T(8,128)(2,1)} %param.37) | copy-start | bytes 3145732
  211.1 4.4 %copy-start.6 = (f32[128,2]{0,1:T(2,128)S(1)}, f32[128,2]{0,1:T(2,128)}, u32[]{:S(2)}) copy-start(f32[128,2]{0,1:T(2,128)} %param.36) | copy-start | bytes 3076
  211.1 4.5 %copy-start.8 = (f32[128]{0:T(128)S(1)}, f32[128]{0:T(128)}, u32[]{:S(2)}) copy-start(f32[128]{0:T(128)} %param.35) | copy-start | bytes 1540
  211.1 53.1 %all-to-all-start.2 = ((bf16[16,32,16,128]{3,2,1,0:T(8,128)(2,1)}), bf16[16,32,16,128]{3,2,1,0:T(8,128)(2,1)S(1)}, u32[]{:S(2)}, u32[]{:S(2)}) async-start(bf16[16,32,16,128]{3,2,1,0:T(8,128)(2,1)} %bitcast.260), calls=%async_computation.2 | async-start | bytes 4194304 | tf_op jit(solution)/shard_map/all_to_all | solution.py:91
  265.1 14.7 %all-to-all-start.3 = ((bf16[32,16,128]{2,1,0:T(8,128)(2,1)}), bf16[32,16,128]{2,1,0:T(8,128)(2,1)S(1)}, u32[]{:S(2)}, u32[]{:S(2)}) async-start(bf16[32,16,128]{2,1,0:T(8,128)(2,1)} %reduce_sum.69), calls=%async_computation.3 | async-start | bytes 262144 | tf_op jit(solution)/shard_map/all_to_all | solution.py:260
